TPU v7x, 32 devices: a whole 2x2x4 slice. The times are simulated.
32 devices in a mesh: rep: 2 (over x), fs: 8 (over z, y), tp: 2 (over core).
Axes of the slice: x: 2, y: 2, z: 4, core: 2. Of those that a mesh axis runs over, the one named last changes fastest.
Arguments:
- tokens: bfloat16 [8192, 2048], P(('rep', 'fs')), may hold values from -6 to 6
- mix_gain: bfloat16 [2048], replicated, may hold values from 0.099609375 to 1.8984375
- value_weight: bfloat16 [2048, 1536], P('fs', 'tp'), may hold values from -0.125 to 0.125
- outer_gate_weight: bfloat16 [2048, 1536], P('fs', 'tp'), may hold values from -0.125 to 0.125
- inner_gate_weight: bfloat16 [2048, 1536], P('fs', 'tp'), may hold values from -0.125 to 0.125
- conv_taps: bfloat16 [3, 1536], P(None, 'tp'), may hold values from -3 to 3
- mix_out_weight: bfloat16 [1536, 2048], P('tp', 'fs'), may hold values from -0.15625 to 0.15625
- ffn_gain: bfloat16 [2048], replicated, may hold values from 0.099609375 to 1.8984375
- gate_weight: bfloat16 [2048, 4096], P('fs', 'tp'), may hold values from -0.125 to 0.125
- up_weight: bfloat16 [2048, 4096], P('fs', 'tp'), may hold values from -0.125 to 0.125
- down_weight: bfloat16 [4096, 2048], P('tp', 'fs'), may hold values from -0.09375 to 0.09375
Outputs:
- layer_out: bfloat16 [8192, 2048], P(('rep', 'fs'))
All inputs are finite; a program needn't handle non-finite values.
Results may differ from a plain program's by a relative error of at most 0.02.
Values may be sent and summed in bfloat16 or wider, within the bound.
A program may use at most 128 MiB of HBM per device.

v0:
```python
import jax
import jax.numpy as jnp
from jax import lax
from jax.sharding import PartitionSpec as P

SEQ_GRP = 2
EPS = 1e-05


def rms_norm(values, gain):
    floats = values.astype(jnp.float32)
    scaled = floats * lax.rsqrt(jnp.mean(floats * floats, axis=-1, keepdims=True) + EPS)
    return (scaled * gain.astype(jnp.float32)).astype(jnp.bfloat16)


def short_conv(value_proj, outer_proj, inner_proj, conv_taps, seq_len):
    mixed_in = inner_proj.astype(jnp.float32) * value_proj.astype(jnp.float32)
    count_rows = mixed_in.shape[0]
    position = (jnp.arange(count_rows, dtype=jnp.int32) % seq_len)[:, None]
    zero_row = jnp.zeros((1, mixed_in.shape[1]), jnp.float32)
    back_one = jnp.where(position >= 1, jnp.concatenate([zero_row, mixed_in[:-1]], axis=0), 0.0)
    back_two = jnp.where(
        position >= 2, jnp.concatenate([zero_row, zero_row, mixed_in[:-2]], axis=0), 0.0
    )
    taps = conv_taps.astype(jnp.float32)
    convolved = taps[0] * back_two + taps[1] * back_one + taps[2] * mixed_in
    return (outer_proj.astype(jnp.float32) * convolved).astype(jnp.bfloat16)


def local(
    tokens,
    mix_gain,
    value_weight,
    outer_gate_weight,
    inner_gate_weight,
    conv_taps,
    mix_out_weight,
    ffn_gain,
    gate_weight,
    up_weight,
    down_weight,
):
    row_count = tokens.shape[0]
    share = row_count // lax.axis_size("tp")
    seq_len = row_count // SEQ_GRP
    own_rows = lax.dynamic_slice_in_dim(tokens, lax.axis_index("tp") * share, share, 0).astype(
        jnp.float32
    )
    normed = rms_norm(tokens, mix_gain)
    value_full, outer_full, inner_full, mix_out_full, gate_full, up_full, down_full = (
        lax.all_gather(value_weight, "fs", axis=0, tiled=True),
        lax.all_gather(outer_gate_weight, "fs", axis=0, tiled=True),
        lax.all_gather(inner_gate_weight, "fs", axis=0, tiled=True),
        lax.all_gather(mix_out_weight, "fs", axis=1, tiled=True),
        lax.all_gather(gate_weight, "fs", axis=0, tiled=True),
        lax.all_gather(up_weight, "fs", axis=0, tiled=True),
        lax.all_gather(down_weight, "fs", axis=1, tiled=True),
    )
    value_proj = jnp.dot(normed, value_full, preferred_element_type=jnp.float32).astype(
        jnp.bfloat16
    )
    outer_proj = jnp.dot(normed, outer_full, preferred_element_type=jnp.float32).astype(
        jnp.bfloat16
    )
    inner_proj = jnp.dot(normed, inner_full, preferred_element_type=jnp.float32).astype(
        jnp.bfloat16
    )
    mixed = short_conv(value_proj, outer_proj, inner_proj, conv_taps, seq_len)
    picked = mixed
    mix_total = lax.psum_scatter(
        jnp.dot(picked, mix_out_full, preferred_element_type=jnp.float32).astype(jnp.bfloat16),
        "tp",
        scatter_dimension=0,
        tiled=True,
    ).astype(jnp.float32)
    after_mix = (own_rows + mix_total).astype(jnp.bfloat16)
    normed_two = rms_norm(after_mix, ffn_gain)
    block_rows = lax.all_gather(normed_two, "tp", axis=0, tiled=True)
    gate_proj = jnp.dot(block_rows, gate_full, preferred_element_type=jnp.float32)
    up_proj = jnp.dot(block_rows, up_full, preferred_element_type=jnp.float32)
    hidden = (jax.nn.silu(gate_proj) * up_proj).astype(jnp.bfloat16)
    picked = hidden
    ffn_total = lax.psum_scatter(
        jnp.dot(picked, down_full, preferred_element_type=jnp.float32).astype(jnp.bfloat16),
        "tp",
        scatter_dimension=0,
        tiled=True,
    ).astype(jnp.float32)
    finished = (after_mix.astype(jnp.float32) + ffn_total).astype(jnp.bfloat16)
    return lax.all_gather(finished, "tp", axis=0, tiled=True)


def solution(mesh):
    placed = (
        P(("rep", "fs"), None),
        P(),
        P("fs", "tp"),
        P("fs", "tp"),
        P("fs", "tp"),
        P(None, "tp"),
        P("tp", "fs"),
        P(),
        P("fs", "tp"),
        P("fs", "tp"),
        P("tp", "fs"),
    )
    return jax.shard_map(
        local, mesh=mesh, in_specs=placed, out_specs=P(("rep", "fs"), None), check_vma=False
    )
```

profile of v0, /device:TPU:0, one launch (start us, length us, event | category | flops | bytes accessed | tf_op | source)
XLA Modules:
  0.0 718.0 jit_solution(16249208888733937228)
XLA Ops:
  6.5 0.7 all-gather.14.cloned.1.call-update
  7.3 0.7 all-gather.12.cloned.1.call-update
  8.1 0.7 all-gather.10.cloned.1.call-update
  8.8 0.5 all-gather.16.cloned.1.call-update
  9.4 0.7 convert_element_type.69
  10.1 0.7 convert_element_type.73
  10.8 2.1 fusion
  12.9 59.4 %all-gather.14.cloned.1.call-done = bf16[2048,768]{1,0:T(8,128)(2,1)} async-done(((bf16[256,768]{1,0:T(8,128)(2,1)}), bf16[2048,768]{1,0:T(8,128)(2,1)}) %all-gather.14.cloned.1.call-update) | async-done | bytes 3145744 | tf_op jit(solution)/shard_map/all_gather | solution.py:51
  72.3 3.7 convolution_convert_fusion.2
  76.0 57.2 %all-gather.12.cloned.1.call-done = bf16[2048,768]{1,0:T(8,128)(2,1)} async-done(((bf16[256,768]{1,0:T(8,128)(2,1)}), bf16[2048,768]{1,0:T(8,128)(2,1)}) %all-gather.12.cloned.1.call-update) | async-done | bytes 3145744 | tf_op jit(solution)/shard_map/all_gather | solution.py:53
  133.2 4.9 convert_multiply_fusion.4
  138.1 56.0 %all-gather.10.cloned.1.call-done = bf16[2048,768]{1,0:T(8,128)(2,1)} async-done(((bf16[256,768]{1,0:T(8,128)(2,1)}), bf16[2048,768]{1,0:T(8,128)(2,1)}) %all-gather.10.cloned.1.call-update) | async-done | bytes 3145744 | tf_op jit(solution)/shard_map/all_gather | solution.py:52
  194.1 63.2 %all-gather.16.cloned.1.call-done = bf16[768,2048]{1,0:T(8,128)(2,1)} async-done(((bf16[768,256]{1,0:T(8,128)(2,1)}), bf16[768,2048]{1,0:T(8,128)(2,1)}) %all-gather.16.cloned.1.call-update) | async-done | bytes 3145744 | tf_op jit(solution)/shard_map/all_gather | solution.py:54
  257.3 9.8 %convolution_convert_fusion.1 = bf16[512,2048]{1,0:T(8,128)(2,1)} fusion(bf16[768,2048]{1,0:T(8,128)(2,1)} %all-gather.16.cloned.1.call-done, f32[512,768]{1,0:T(8,128)} %convert_multiply_fusion.4, f32[511,768]{1,0:T(8,128)} %bitcast.20, f32[510,768]{1,0:T(8,128)} %bitcast.21, bf16[2048,768]{1,0:T(8,128)(2,1)} %all-gather.10.cloned.1.call-done, ...), kind=kOutput, calls=%fused_computation.10 | convolution fusion | flops 3230793728 | bytes 15215616 | tf_op jit(solution)/shard_map/dot_general | solution.py:71
  267.2 0.6 copy-done.1
  267.8 7.4 %reduce-scatter.3.cloned.1.call-done = bf16[256,2048]{1,0:T(8,128)(2,1)} async-done(((bf16[512,2048]{1,0:T(8,128)(2,1)}), bf16[256,2048]{1,0:T(8,128)(2,1)}) %reduce-scatter.3.cloned.1.call-update) | async-done | bytes 1048592 | tf_op jit(solution)/shard_map/reduce_scatter | solution.py:70
  275.3 1.7 fusion.3
  277.0 1.3 fusion.5
  278.4 0.7 all-gather.20.cloned.1.call-update
  279.1 0.7 all-gather.22.cloned.1.call-update
  279.9 0.7 all-gather.24.cloned.1.call-update
  280.6 0.2 reduce-scatter.5.cloned.1.call-start
  280.8 9.6 %all-gather.18.cloned.1.call-done = bf16[512,2048]{1,0:T(8,128)(2,1)} async-done(((bf16[256,2048]{1,0:T(8,128)(2,1)}), bf16[512,2048]{1,0:T(8,128)(2,1)}) %all-gather.18.cloned.1.call-update) | async-done | bytes 2097168 | tf_op jit(solution)/shard_map/all_gather | solution.py:78
  290.4 127.8 %all-gather.20.cloned.1.call-done = bf16[2048,2048]{1,0:T(8,128)(2,1)} async-done(((bf16[256,2048]{1,0:T(8,128)(2,1)}), bf16[2048,2048]{1,0:T(8,128)(2,1)}) %all-gather.20.cloned.1.call-update) | async-done | bytes 8388624 | tf_op jit(solution)/shard_map/all_gather | solution.py:55
  418.2 10.5 %fusion.17 = f32[512,2048]{1,0:T(8,128)} fusion(bf16[512,2048]{1,0:T(8,128)(2,1)} %all-gather.18.cloned.1.call-done, bf16[2048,2048]{1,0:T(8,128)(2,1)} %all-gather.20.cloned.1.call-done), kind=kOutput, calls=%fused_computation.34 | convolution fusion | flops 4294967296 | bytes 14680064 | tf_op jit(solution)/shard_map/dot_general | solution.py:79
  428.6 114.3 %all-gather.22.cloned.1.call-done = bf16[2048,2048]{1,0:T(8,128)(2,1)} async-done(((bf16[256,2048]{1,0:T(8,128)(2,1)}), bf16[2048,2048]{1,0:T(8,128)(2,1)}) %all-gather.22.cloned.1.call-update) | async-done | bytes 8388624 | tf_op jit(solution)/shard_map/all_gather | solution.py:56
  543.0 125.2 %all-gather.24.cloned.1.call-done = bf16[2048,2048]{1,0:T(8,128)(2,1)} async-done(((bf16[2048,256]{1,0:T(8,128)(2,1)}), bf16[2048,2048]{1,0:T(8,128)(2,1)}) %all-gather.24.cloned.1.call-update) | async-done | bytes 8388624 | tf_op jit(solution)/shard_map/all_gather | solution.py:57
  668.2 17.4 %convolution_convert_fusion = bf16[512,2048]{1,0:T(8,128)(2,1)} fusion(bf16[2048,2048]{1,0:T(8,128)(2,1)} %all-gather.24.cloned.1.call-done, f32[512,2048]{1,0:T(8,128)} %fusion.17, bf16[512,2048]{1,0:T(8,128)(2,1)S(1)} %copy-done.2, bf16[2048,2048]{1,0:T(8,128)(2,1)} %all-gather.22.cloned.1.call-done), kind=kOutput, calls=%fused_computation.9 | convolution fusion | flops 8597274624 | bytes 25165824 | tf_op jit(solution)/shard_map/dot_general | solution.py:84
  685.7 8.0 %reduce-scatter.5.cloned.1.call-done = bf16[256,2048]{1,0:T(8,128)(2,1)} async-done(((bf16[512,2048]{1,0:T(8,128)(2,1)}), bf16[256,2048]{1,0:T(8,128)(2,1)}) %reduce-scatter.5.cloned.1.call-update) | async-done | bytes 1048592 | tf_op jit(solution)/shard_map/reduce_scatter | solution.py:83
  693.7 2.6 fusion.6
  696.3 12.0 %all-gather.26.cloned.1.call-done = bf16[512,2048]{1,0:T(8,128)(2,1)} async-done(((bf16[256,2048]{1,0:T(8,128)(2,1)}), bf16[512,2048]{1,0:T(8,128)(2,1)}) %all-gather.26.cloned.1.call-update) | async-done | bytes 2097168 | tf_op jit(solution)/shard_map/all_gather | solution.py:90
  708.3 3.2 copy.13
  (24 shorter events, 0.5 us)
Async XLA Ops:
  6.5 65.8 %copy-start = (bf16[512,2048]{1,0:T(8,128)(2,1)S(1)}, bf16[512,2048]{1,0:T(8,128)(2,1)}, u32[]{:S(2)}) copy-start(bf16[512,2048]{1,0:T(8,128)(2,1)} %param.11) | copy-start | bytes 6291460
  6.5 65.8 %all-gather.14.cloned.1.call-start = ((), (), s32[]{:S(2)}) async-start(), calls=%async_computation.4 | async-start | bytes 3538944 | tf_op jit(solution)/shard_map/all_gather | solution.py:51
  7.3 125.9 %all-gather.12.cloned.1.call-start = ((), (), s32[]{:S(2)}) async-start(), calls=%async_computation.3 | async-start | bytes 3538944 | tf_op jit(solution)/shard_map/all_gather | solution.py:53
  8.0 186.1 %all-gather.10.cloned.1.call-start = ((), (), s32[]{:S(2)}) async-start(), calls=%async_computation.2 | async-start | bytes 3538944 | tf_op jit(solution)/shard_map/all_gather | solution.py:52
  8.7 248.6 %all-gather.16.cloned.1.call-start = ((), (), s32[]{:S(2)}) async-start(), calls=%async_computation.5 | async-start | bytes 3538944 | tf_op jit(solution)/shard_map/all_gather | solution.py:54
  9.3 266.0 %reduce-scatter.3.cloned.1.call-start = ((), (), s32[]{:S(2)}) async-start(), calls=%async_computation.6 | async-start | bytes 3145728 | tf_op jit(solution)/shard_map/reduce_scatter | solution.py:70
  267.2 0.7 copy-start.1
  267.2 23.2 %all-gather.18.cloned.1.call-start = ((), (), s32[]{:S(2)}) async-start(), calls=%async_computation.7 | async-start | bytes 3145728 | tf_op jit(solution)/shard_map/all_gather | solution.py:78
  278.3 139.8 %all-gather.20.cloned.1.call-start = ((), (), s32[]{:S(2)}) async-start(), calls=%async_computation.8 | async-start | bytes 9437184 | tf_op jit(solution)/shard_map/all_gather | solution.py:55
  279.1 263.9 %all-gather.22.cloned.1.call-start = ((), (), s32[]{:S(2)}) async-start(), calls=%async_computation.9 | async-start | bytes 9437184 | tf_op jit(solution)/shard_map/all_gather | solution.py:56
  279.8 388.3 %all-gather.24.cloned.1.call-start = ((), (), s32[]{:S(2)}) async-start(), calls=%async_computation.10 | async-start | bytes 9437184 | tf_op jit(solution)/shard_map/all_gather | solution.py:57
  280.6 413.1 %reduce-scatter.5.cloned.1.call-start = ((), (), s32[]{:S(2)}) async-start(), calls=%async_computation.11 | async-start | bytes 3145728 | tf_op jit(solution)/shard_map/reduce_scatter | solution.py:83
  290.4 377.8 %copy-start.2 = (bf16[512,2048]{1,0:T(8,128)(2,1)S(1)}, bf16[512,2048]{1,0:T(8,128)(2,1)}, u32[]{:S(2)}) copy-start(bf16[512,2048]{1,0:T(8,128)(2,1)} %all-gather.18.cloned.1.call-done) | copy-start | bytes 6291460
  685.6 22.7 %all-gather.26.cloned.1.call-start = ((), (), s32[]{:S(2)}) async-start(), calls=%async_computation.12 | async-start | bytes 3145728 | tf_op jit(solution)/shard_map/all_gather | solution.py:90
Sparse Core Ops, SparseCore 0:
  9.5 62.7 all-gather.13
  74.5 58.6 all-gather.11
  135.4 58.6 all-gather.9
  196.0 61.3 all-gather.15
  267.3 7.9 reduce-scatter.2
  278.5 11.8 all-gather.17
  292.5 125.6 all-gather.19
  420.3 122.6 all-gather.21
  545.0 123.1 all-gather.23
  685.7 7.9 reduce-scatter.4
  696.4 11.8 all-gather.25
where the time goes:
time: 718 us
  waiting for transfers between devices  645 us (90%)
  matrix products  46.3 us (6%)
  between operations  13.3 us (2%)
  other arithmetic  9.09 us (1%)
    all_gather x1, waiting for transfers between devices, local(): lax.all_gather(gate_weight, 'fs', axis=0, tiled=True)  128 us
    all_gather x1, waiting for transfers between devices, local(): lax.all_gather(down_weight, 'fs', axis=1, tiled=True)  125 us
    all_gather x1, waiting for transfers between devices, local(): lax.all_gather(up_weight, 'fs', axis=0, tiled=True)  114 us
    all_gather x1, waiting for transfers between devices, local(): lax.all_gather(mix_out_weight, 'fs', axis=1, tiled=True)  63.2 us
    all_gather x1, waiting for transfers between devices, local(): lax.all_gather(value_weight, 'fs', axis=0, tiled=True)  59.4 us
    all_gather x1, waiting for transfers between devices, local(): lax.all_gather(inner_gate_weight, 'fs', axis=0, tiled=True)  57.2 us
    all_gather x1, waiting for transfers between devices, local(): lax.all_gather(outer_gate_weight, 'fs', axis=0, tiled=True)  56 us
    dot_general x1, matrix products, local(): jnp.dot(picked, down_full, preferred_element_type=jnp.float32)  17.4 us
  transfers between devices with their start and end apart: 11, of which 11 were waited for; matrix products, arithmetic and copies ran while one was open for 3% of the time, Pallas kernels for 0%

commit v1 on v0

--- a/solution.py
+++ b/solution.py
@@ -5,6 +5,14 @@
 
 SEQ_GRP = 2
 EPS = 1e-05
+
+
+def fit_set_for(body, array_dim):
+    body = jnp.moveaxis(body, 0, array_dim)
+    near = body.shape
+    return body.reshape(
+        *near[:array_dim], near[array_dim] * near[array_dim + 1], *near[array_dim + 2 :]
+    )
 
 
 def rms_norm(values, gain):
@@ -40,6 +48,32 @@
     up_weight,
     down_weight,
 ):
+
+    def number_field(vals, peer_axis, along_dim):
+        p_count = jax.lax.axis_size(peer_axis)
+        r2 = range(p_count)
+        f_next = map(lambda u: (u, (u + 1) % p_count), r2)
+        grid = list(f_next)
+        piece_next, reached = ([], [])
+        kept_rows = [(dd, d) for d, dd in grid]
+        for no in tuple(range(p_count - 1)):
+            if no % 2 == 0:
+                b_next = jax.lax.ppermute(
+                    piece_next[-1] if piece_next else vals, axis_name=peer_axis, perm=grid
+                )
+                piece_next.append(b_next)
+            else:
+                row_out = jax.lax.ppermute(
+                    reached[-1] if reached else vals, peer_axis, perm=kept_rows
+                )
+                reached.append(row_out)
+        a_next = jnp.stack([*piece_next[::-1], vals, *reached])
+        odd = len(piece_next)
+        kept_arr = jax.lax.axis_index(peer_axis)
+        front = kept_arr - odd
+        a_next = a_next[(jnp.arange(p_count) - front) % p_count]
+        return fit_set_for(a_next, along_dim)
+
     row_count = tokens.shape[0]
     share = row_count // lax.axis_size("tp")
     seq_len = row_count // SEQ_GRP
@@ -50,7 +84,7 @@
     value_full, outer_full, inner_full, mix_out_full, gate_full, up_full, down_full = (
         lax.all_gather(value_weight, "fs", axis=0, tiled=True),
         lax.all_gather(outer_gate_weight, "fs", axis=0, tiled=True),
-        lax.all_gather(inner_gate_weight, "fs", axis=0, tiled=True),
+        number_field(inner_gate_weight, "fs", 0),
         lax.all_gather(mix_out_weight, "fs", axis=1, tiled=True),
         lax.all_gather(gate_weight, "fs", axis=0, tiled=True),
         lax.all_gather(up_weight, "fs", axis=0, tiled=True),

time: 718 us -> 696 us (0.969)
  waiting for transfers between devices: 645 us -> 599 us
  starting transfers between devices: 0.57 us -> 16.9 us
  local copies, waits for them, and re-layouts: 3.81 us -> 13.9 us
    ppermute x0 -> x7, waiting for transfers between devices: none -> 68.8 us  [the longest x4 61 us: number_field(): jax.lax.ppermute(piece_next[-1] if piece_next else vals, axis_name=peer_a...]
    all_gather x1 -> x0, waiting for transfers between devices: 57.2 us -> none  [local(): lax.all_gather(inner_gate_weight, 'fs', axis=0, tiled=True)]
    all_gather x1, waiting for transfers between devices: 59.4 us -> 2.43 us  [local(): lax.all_gather(value_weight, 'fs', axis=0, tiled=True)]
    ppermute x0 -> x7, starting transfers between devices: none -> 16.4 us  [the longest x3 10.9 us: number_field(): jax.lax.ppermute(reached[-1] if reached else vals, peer_axis, perm=kept_r...]
  transfers between devices with their start and end apart: 11 -> 17, of which waited for: 11 -> 15; matrix products, arithmetic and copies ran while one was open for 3% -> 4% of each run, Pallas kernels for 0% -> 0%
where the time goes in v1:
time: 696 us; the launch traced here: 695 us
  waiting for transfers between devices  599 us (86%)
  matrix products  44.6 us (6%)
  starting transfers between devices  16.9 us (2%)
  local copies, waits for them, and re-layouts  13.9 us (2%)
  between operations  13.6 us (2%)
  other arithmetic  7.73 us (1%)
    all_gather x1, waiting for transfers between devices, local(): lax.all_gather(gate_weight, 'fs', axis=0, tiled=True)  128 us
    all_gather x1, waiting for transfers between devices, local(): lax.all_gather(down_weight, 'fs', axis=1, tiled=True)  125 us
    all_gather x1, waiting for transfers between devices, local(): lax.all_gather(up_weight, 'fs', axis=0, tiled=True)  114 us
    ppermute x4, waiting for transfers between devices, number_field(): jax.lax.ppermute(piece_next[-1] if piece_next else vals, axis_name=peer_a...  61 us
    all_gather x1, waiting for transfers between devices, local(): lax.all_gather(outer_gate_weight, 'fs', axis=0, tiled=True)  60.4 us
    all_gather x1, waiting for transfers between devices, local(): lax.all_gather(mix_out_weight, 'fs', axis=1, tiled=True)  57.4 us
    dot_general x1, matrix products, local(): jnp.dot(picked, down_full, preferred_element_type=jnp.float32)  17.4 us
  transfers between devices with their start and end apart: 17, of which 15 were waited for; matrix products, arithmetic and copies ran while one was open for 4% of the time, Pallas kernels for 0%

profile of v1, /device:TPU:0, one launch (start us, length us, event | category | flops | bytes accessed | tf_op | source)
XLA Modules:
  0.0 695.4 jit_solution(5265804674140308043)
XLA Ops:
  8.8 3.0 collective-permute-start
  11.8 12.5 %collective-permute-done = bf16[256,768]{1,0:T(8,128)(2,1)S(1)} collective-permute-done((bf16[256,768]{1,0:T(8,128)(2,1)}, bf16[256,768]{1,0:T(8,128)(2,1)S(1)}, u32[]{:S(2)}, u32[]{:S(2)}) %collective-permute-start) | collective-permute-done | bytes 393248 | tf_op jit(solution)/shard_map/ppermute | solution.py:61
  24.3 4.7 collective-permute-start.4
  29.0 17.7 %collective-permute-done.1 = bf16[256,768]{1,0:T(8,128)(2,1)S(1)} collective-permute-done((bf16[256,768]{1,0:T(8,128)(2,1)S(1)}, bf16[256,768]{1,0:T(8,128)(2,1)S(1)}, u32[]{:S(2)}, u32[]{:S(2)}) %collective-permute-start.1) | collective-permute-done | bytes 393248 | tf_op jit(solution)/shard_map/ppermute | solution.py:61
  46.8 2.1 fusion
  48.9 4.8 collective-permute-start.5
  53.7 18.2 %collective-permute-done.2 = bf16[256,768]{1,0:T(8,128)(2,1)S(1)} collective-permute-done((bf16[256,768]{1,0:T(8,128)(2,1)S(1)}, bf16[256,768]{1,0:T(8,128)(2,1)S(1)}, u32[]{:S(2)}, u32[]{:S(2)}) %collective-permute-start.2) | collective-permute-done | bytes 393248 | tf_op jit(solution)/shard_map/ppermute | solution.py:61
  71.8 2.5 collective-permute-start.3
  74.4 7.8 %collective-permute-done.5 = bf16[256,768]{1,0:T(8,128)(2,1)S(1)} collective-permute-done((bf16[256,768]{1,0:T(8,128)(2,1)S(1)}, bf16[256,768]{1,0:T(8,128)(2,1)S(1)}, u32[]{:S(2)}, u32[]{:S(2)}) %collective-permute-start.5) | collective-permute-done | bytes 393248 | tf_op jit(solution)/shard_map/ppermute | solution.py:66
  82.2 1.4 collective-permute-start.6
  83.6 12.6 %collective-permute-done.3 = bf16[256,768]{1,0:T(8,128)(2,1)S(1)} collective-permute-done((bf16[256,768]{1,0:T(8,128)(2,1)S(1)}, bf16[256,768]{1,0:T(8,128)(2,1)S(1)}, u32[]{:S(2)}, u32[]{:S(2)}) %collective-permute-start.3) | collective-permute-done | bytes 393248 | tf_op jit(solution)/shard_map/ppermute | solution.py:61
  96.2 0.8 bitcast_dynamic-update-slice_fusion.7
  102.5 4.4 gather_fusion
  107.0 2.4 all-gather.11.cloned.1.call-done
  109.4 3.9 convolution_convert_fusion.2
  113.3 3.1 convert_multiply_fusion.4
  116.4 57.4 %all-gather.13.cloned.1.call-done = bf16[768,2048]{1,0:T(8,128)(2,1)} async-done(((bf16[768,256]{1,0:T(8,128)(2,1)}), bf16[768,2048]{1,0:T(8,128)(2,1)}) %all-gather.13.cloned.1.call-update) | async-done | bytes 3145744 | tf_op jit(solution)/shard_map/all_gather | solution.py:88
  173.8 60.4 %all-gather.9.cloned.1.call-done = bf16[2048,768]{1,0:T(8,128)(2,1)} async-done(((bf16[256,768]{1,0:T(8,128)(2,1)}), bf16[2048,768]{1,0:T(8,128)(2,1)}) %all-gather.9.cloned.1.call-update) | async-done | bytes 3145744 | tf_op jit(solution)/shard_map/all_gather | solution.py:86
  234.2 9.8 %convolution_convert_fusion.1 = bf16[512,2048]{1,0:T(8,128)(2,1)} fusion(bf16[768,2048]{1,0:T(8,128)(2,1)} %all-gather.13.cloned.1.call-done, f32[512,768]{1,0:T(8,128)} %convert_multiply_fusion.4, f32[511,768]{1,0:T(8,128)} %bitcast.40, f32[510,768]{1,0:T(8,128)} %bitcast.41, bf16[2048,768]{1,0:T(8,128)(2,1)} %all-gather.9.cloned.1.call-done, ...), kind=kOutput, calls=%fused_computation.11 | convolution fusion | flops 3230793728 | bytes 15215616 | tf_op jit(solution)/shard_map/dot_general | solution.py:105
  244.1 8.5 %reduce-scatter.3.cloned.1.call-done = bf16[256,2048]{1,0:T(8,128)(2,1)} async-done(((bf16[512,2048]{1,0:T(8,128)(2,1)}), bf16[256,2048]{1,0:T(8,128)(2,1)}) %reduce-scatter.3.cloned.1.call-update) | async-done | bytes 1048592 | tf_op jit(solution)/shard_map/reduce_scatter | solution.py:104
  252.6 1.7 fusion.3
  254.3 1.3 fusion.5
  257.9 9.7 %all-gather.15.cloned.1.call-done = bf16[512,2048]{1,0:T(8,128)(2,1)} async-done(((bf16[256,2048]{1,0:T(8,128)(2,1)}), bf16[512,2048]{1,0:T(8,128)(2,1)}) %all-gather.15.cloned.1.call-update) | async-done | bytes 2097168 | tf_op jit(solution)/shard_map/all_gather | solution.py:112
  267.6 127.7 %all-gather.17.cloned.1.call-done = bf16[2048,2048]{1,0:T(8,128)(2,1)} async-done(((bf16[256,2048]{1,0:T(8,128)(2,1)}), bf16[2048,2048]{1,0:T(8,128)(2,1)}) %all-gather.17.cloned.1.call-update) | async-done | bytes 8388624 | tf_op jit(solution)/shard_map/all_gather | solution.py:89
  395.3 10.5 %fusion.19 = f32[512,2048]{1,0:T(8,128)} fusion(bf16[512,2048]{1,0:T(8,128)(2,1)} %all-gather.15.cloned.1.call-done, bf16[2048,2048]{1,0:T(8,128)(2,1)} %all-gather.17.cloned.1.call-done), kind=kOutput, calls=%fused_computation.50 | convolution fusion | flops 4294967296 | bytes 14680064 | tf_op jit(solution)/shard_map/dot_general | solution.py:113
  405.8 114.3 %all-gather.19.cloned.1.call-done = bf16[2048,2048]{1,0:T(8,128)(2,1)} async-done(((bf16[256,2048]{1,0:T(8,128)(2,1)}), bf16[2048,2048]{1,0:T(8,128)(2,1)}) %all-gather.19.cloned.1.call-update) | async-done | bytes 8388624 | tf_op jit(solution)/shard_map/all_gather | solution.py:90
  520.1 125.2 %all-gather.21.cloned.1.call-done = bf16[2048,2048]{1,0:T(8,128)(2,1)} async-done(((bf16[2048,256]{1,0:T(8,128)(2,1)}), bf16[2048,2048]{1,0:T(8,128)(2,1)}) %all-gather.21.cloned.1.call-update) | async-done | bytes 8388624 | tf_op jit(solution)/shard_map/all_gather | solution.py:91
  645.3 17.4 %convolution_convert_fusion = bf16[512,2048]{1,0:T(8,128)(2,1)} fusion(bf16[2048,2048]{1,0:T(8,128)(2,1)} %all-gather.21.cloned.1.call-done, f32[512,2048]{1,0:T(8,128)} %fusion.19, bf16[512,2048]{1,0:T(8,128)(2,1)S(1)} %copy-done.6, bf16[2048,2048]{1,0:T(8,128)(2,1)} %all-gather.19.cloned.1.call-done), kind=kOutput, calls=%fused_computation.10 | convolution fusion | flops 8597274624 | bytes 25165824 | tf_op jit(solution)/shard_map/dot_general | solution.py:118
  662.8 8.0 %reduce-scatter.5.cloned.1.call-done = bf16[256,2048]{1,0:T(8,128)(2,1)} async-done(((bf16[512,2048]{1,0:T(8,128)(2,1)}), bf16[256,2048]{1,0:T(8,128)(2,1)}) %reduce-scatter.5.cloned.1.call-update) | async-done | bytes 1048592 | tf_op jit(solution)/shard_map/reduce_scatter | solution.py:117
  670.8 2.6 fusion.6
  673.4 12.0 %all-gather.23.cloned.1.call-done = bf16[512,2048]{1,0:T(8,128)(2,1)} async-done(((bf16[256,2048]{1,0:T(8,128)(2,1)}), bf16[512,2048]{1,0:T(8,128)(2,1)}) %all-gather.23.cloned.1.call-update) | async-done | bytes 2097168 | tf_op jit(solution)/shard_map/all_gather | solution.py:124
  685.5 3.2 copy.20
  (54 shorter events, 10.2 us)
Async XLA Ops:
  6.5 67.8 %copy-start.4 = (bf16[2048]{0:T(1024)(128)(2,1)S(1)}, bf16[2048]{0:T(1024)(128)(2,1)}, u32[]{:S(2)}) copy-start(bf16[2048]{0:T(1024)(128)(2,1)} %param.12) | copy-start | bytes 12292
  6.5 67.8 %copy-start.3 = (bf16[3,768]{1,0:T(4,128)(2,1)S(1)}, bf16[3,768]{1,0:T(4,128)(2,1)}, u32[]{:S(2)}) copy-start(bf16[3,768]{1,0:T(4,128)(2,1)} %param.16) | copy-start | bytes 13828
  6.5 102.9 %all-gather.11.cloned.1.call-start = ((), (), s32[]{:S(2)}) async-start(), calls=%async_computation.3 | async-start | bytes 3538944 | tf_op jit(solution)/shard_map/all_gather | solution.py:85
  7.3 92.1 %copy-start.2 = (bf16[256,768]{1,0:T(8,128)(2,1)S(1)}, bf16[256,768]{1,0:T(8,128)(2,1)}, u32[]{:S(2)}) copy-start(bf16[256,768]{1,0:T(8,128)(2,1)} %param.15) | copy-start | bytes 1179652
  7.3 166.5 %all-gather.13.cloned.1.call-start = ((), (), s32[]{:S(2)}) async-start(), calls=%async_computation.4 | async-start | bytes 3538944 | tf_op jit(solution)/shard_map/all_gather | solution.py:88
  8.0 226.2 %all-gather.9.cloned.1.call-start = ((), (), s32[]{:S(2)}) async-start(), calls=%async_computation.2 | async-start | bytes 3538944 | tf_op jit(solution)/shard_map/all_gather | solution.py:86
  8.8 243.8 %reduce-scatter.3.cloned.1.call-start = ((), (), s32[]{:S(2)}) async-start(), calls=%async_computation.5 | async-start | bytes 3145728 | tf_op jit(solution)/shard_map/reduce_scatter | solution.py:104
  8.8 15.5 %collective-permute-start = (bf16[256,768]{1,0:T(8,128)(2,1)}, bf16[256,768]{1,0:T(8,128)(2,1)S(1)}, u32[]{:S(2)}, u32[]{:S(2)}) collective-permute-start(bf16[256,768]{1,0:T(8,128)(2,1)} %param.15), channel_id=1, source_target_pairs={{0,2},{2,4},{4,6},{6,8},{8,10},{10,12},{12,14},{14,0},{1,3},{3,5},... | collective-permute-start | bytes 1179656 | tf_op jit(solution)/shard_map/ppermute | solution.py:61
  24.3 22.5 %collective-permute-start.1 = (bf16[256,768]{1,0:T(8,128)(2,1)S(1)}, bf16[256,768]{1,0:T(8,128)(2,1)S(1)}, u32[]{:S(2)}, u32[]{:S(2)}) collective-permute-start(bf16[256,768]{1,0:T(8,128)(2,1)S(1)} %collective-permute-done), channel_id=1, source_target_pairs={{0,2},{2,4},{4,6},{6,8},{8,10},{10,12},{12,14},{14,0},{1,3},{3,5},... | collective-permute-start | bytes 1179656 | tf_op jit(solution)/shard_map/ppermute | solution.py:61
  24.3 24.6 %collective-permute-start.4 = (bf16[256,768]{1,0:T(8,128)(2,1)}, bf16[256,768]{1,0:T(8,128)(2,1)S(1)}, u32[]{:S(2)}, u32[]{:S(2)}) collective-permute-start(bf16[256,768]{1,0:T(8,128)(2,1)} %param.15), channel_id=1, source_target_pairs={{2,0},{4,2},{6,4},{8,6},{10,8},{12,10},{14,12},{0,14},{3,1},{5,3},... | collective-permute-start | bytes 1179656 | tf_op jit(solution)/shard_map/ppermute | solution.py:66
  46.8 25.0 %collective-permute-start.2 = (bf16[256,768]{1,0:T(8,128)(2,1)S(1)}, bf16[256,768]{1,0:T(8,128)(2,1)S(1)}, u32[]{:S(2)}, u32[]{:S(2)}) collective-permute-start(bf16[256,768]{1,0:T(8,128)(2,1)S(1)} %collective-permute-done.1), channel_id=1, source_target_pairs={{0,2},{2,4},{4,6},{6,8},{8,10},{10,12},{12,14},{14,0},{1,3},{3,5},... | collective-permute-start | bytes 1179656 | tf_op jit(solution)/shard_map/ppermute | solution.py:61
  48.9 33.4 %collective-permute-start.5 = (bf16[256,768]{1,0:T(8,128)(2,1)S(1)}, bf16[256,768]{1,0:T(8,128)(2,1)S(1)}, u32[]{:S(2)}, u32[]{:S(2)}) collective-permute-start(bf16[256,768]{1,0:T(8,128)(2,1)S(1)} %collective-permute-done.4), channel_id=1, source_target_pairs={{2,0},{4,2},{6,4},{8,6},{10,8},{12,10},{14,12},{0,14},{3,1},{5,3},... | collective-permute-start | bytes 1179656 | tf_op jit(solution)/shard_map/ppermute | solution.py:66
  71.8 24.4 %collective-permute-start.3 = (bf16[256,768]{1,0:T(8,128)(2,1)S(1)}, bf16[256,768]{1,0:T(8,128)(2,1)S(1)}, u32[]{:S(2)}, u32[]{:S(2)}) collective-permute-start(bf16[256,768]{1,0:T(8,128)(2,1)S(1)} %collective-permute-done.2), channel_id=1, source_target_pairs={{0,2},{2,4},{4,6},{6,8},{8,10},{10,12},{12,14},{14,0},{1,3},{3,5},... | collective-permute-start | bytes 1179656 | tf_op jit(solution)/shard_map/ppermute | solution.py:61
  82.2 19.5 %collective-permute-start.6 = (bf16[256,768]{1,0:T(8,128)(2,1)S(1)}, bf16[256,768]{1,0:T(8,128)(2,1)S(1)}, u32[]{:S(2)}, u32[]{:S(2)}) collective-permute-start(bf16[256,768]{1,0:T(8,128)(2,1)S(1)} %collective-permute-done.5), channel_id=1, source_target_pairs={{2,0},{4,2},{6,4},{8,6},{10,8},{12,10},{14,12},{0,14},{3,1},{5,3},... | collective-permute-start | bytes 1179656 | tf_op jit(solution)/shard_map/ppermute | solution.py:66
  102.5 6.9 copy-start
  109.4 3.9 copy-start.1
  234.2 9.9 %copy-start.5 = (bf16[2048]{0:T(1024)(128)(2,1)S(1)}, bf16[2048]{0:T(1024)(128)(2,1)}, u32[]{:S(2)}) copy-start(bf16[2048]{0:T(1024)(128)(2,1)} %param.18) | copy-start | bytes 12292
  244.0 23.6 %all-gather.15.cloned.1.call-start = ((), (), s32[]{:S(2)}) async-start(), calls=%async_computation.6 | async-start | bytes 3145728 | tf_op jit(solution)/shard_map/all_gather | solution.py:112
  255.6 139.7 %all-gather.17.cloned.1.call-start = ((), (), s32[]{:S(2)}) async-start(), calls=%async_computation.7 | async-start | bytes 9437184 | tf_op jit(solution)/shard_map/all_gather | solution.py:89
  256.2 263.9 %all-gather.19.cloned.1.call-start = ((), (), s32[]{:S(2)}) async-start(), calls=%async_computation.8 | async-start | bytes 9437184 | tf_op jit(solution)/shard_map/all_gather | solution.py:90
  257.0 388.3 %all-gather.21.cloned.1.call-start = ((), (), s32[]{:S(2)}) async-start(), calls=%async_computation.9 | async-start | bytes 9437184 | tf_op jit(solution)/shard_map/all_gather | solution.py:91
  257.7 413.1 %reduce-scatter.5.cloned.1.call-start = ((), (), s32[]{:S(2)}) async-start(), calls=%async_computation.10 | async-start | bytes 3145728 | tf_op jit(solution)/shard_map/reduce_scatter | solution.py:117
  267.6 377.7 %copy-start.6 = (bf16[512,2048]{1,0:T(8,128)(2,1)S(1)}, bf16[512,2048]{1,0:T(8,128)(2,1)}, u32[]{:S(2)}) copy-start(bf16[512,2048]{1,0:T(8,128)(2,1)} %all-gather.15.cloned.1.call-done) | copy-start | bytes 6291460
  662.8 22.7 %all-gather.23.cloned.1.call-start = ((), (), s32[]{:S(2)}) async-start(), calls=%async_computation.11 | async-start | bytes 3145728 | tf_op jit(solution)/shard_map/all_gather | solution.py:124
Sparse Core Ops, SparseCore 0:
  9.5 99.8 all-gather.10
  111.5 62.2 all-gather.12
  176.0 58.1 all-gather.8
  244.1 8.4 reduce-scatter.2
  255.8 11.8 all-gather.14
  269.6 125.6 all-gather.16
  397.4 122.6 all-gather.18
  522.2 123.1 all-gather.20
  662.9 7.8 reduce-scatter.4
  673.6 11.8 all-gather.22
